TPU v7x, 32 devices: a whole 2x2x4 slice. The times are simulated.
32 devices in a mesh: fs: 16 (over z, y, x), tp: 2 (over core).
Axes of the slice: x: 2, y: 2, z: 4, core: 2. Of those that a mesh axis runs over, the one named last changes fastest.
Arguments:
- saved_inputs: bfloat16 [2048, 4096], P('fs', 'tp'), may hold values from -6 to 6
- value_cotangent: bfloat16 [2048, 2048], P('fs'), may hold values from -0.1875 to 0.1875
- glu_output: bfloat16 [2048, 2048], P('fs', 'tp'), may hold values from -6 to 6
- conv_cotangent: bfloat16 [2048, 2048], P('fs', 'tp'), may hold values from -0.125 to 0.125
- factor: bfloat16 [4096, 256], P('tp'), may hold values from -0.09375 to 0.09375
- value_weight: float32 [2048, 4096], P('fs', 'tp'), may hold values from -3 to 3
- first_moment: float32 [2048, 256], P('fs', 'tp'), may hold values from -6 to 6
- second_moment: float32 [2048, 256], P('fs', 'tp'), may hold values from 0.25 to 4
- kernel: float32 [31, 2048], P(None, 'tp'), may hold values from -1 to 1
- kernel_first: float32 [31, 2048], P(None, 'tp'), may hold values from -6 to 6
- kernel_second: float32 [31, 2048], P(None, 'tp'), may hold values from 0.25 to 4
Outputs:
- new_value: float32 [2048, 4096], P('fs', 'tp')
- value_copy: bfloat16 [2048, 4096], P('fs', 'tp')
- value_step: float32 [2048, 4096], P('fs', 'tp')
- new_first: float32 [2048, 256], P('fs', 'tp')
- new_second: float32 [2048, 256], P('fs', 'tp')
- new_kernel: float32 [31, 2048], P(None, 'tp')
- new_kernel_first: float32 [31, 2048], P(None, 'tp')
- new_kernel_second: float32 [31, 2048], P(None, 'tp')
All inputs are finite; a program needn't handle non-finite values.
Results may differ from a plain program's by a relative error of at most 0.0055.
Values may be sent and summed in bfloat16 or wider, within the bound.
A program may use at most 64 MiB of HBM per device.

v0:
```python
import jax
import jax.numpy as jnp
from jax import lax
from jax.sharding import PartitionSpec as P

WIDTH = 4096


def from_behind(x, axis, by):
    peers = lax.axis_size(axis)
    pairs = [(i, i + by) for i in range(peers) if 0 <= i + by < peers]
    return lax.ppermute(x, axis, pairs)


def body(
    saved_inputs,
    value_cotangent,
    glu_output,
    conv_cotangent,
    factor,
    value_weight,
    first_moment,
    second_moment,
    kernel,
    kernel_first,
    kernel_second,
):
    highest = lax.Precision.HIGHEST
    factor_f = factor.astype(jnp.float32)
    partial_reduced = jnp.dot(saved_inputs, factor, preferred_element_type=jnp.float32)
    reduced = lax.psum_scatter(
        partial_reduced.astype(jnp.bfloat16), "tp", scatter_dimension=1, tiled=True
    ).astype(jnp.float32)
    upper_part = reduced.astype(jnp.bfloat16)
    lower_part = (reduced - upper_part.astype(jnp.float32)).astype(jnp.bfloat16)
    dims = (((0,), (0,)), ((), ()))
    upper_term = lax.dot_general(
        value_cotangent, upper_part, dims, preferred_element_type=jnp.float32
    )
    lower_term = lax.dot_general(
        value_cotangent, lower_part, dims, preferred_element_type=jnp.float32
    )
    projected = lax.psum_scatter(upper_term + lower_term, "fs", scatter_dimension=0, tiled=True)
    new_first = 0.8 * first_moment + 0.2 * projected
    new_second = 0.9 * second_moment + 0.1 * projected * projected
    direction = new_first / jnp.sqrt(new_second)
    full_direction = lax.all_gather(direction, "tp", axis=1, tiled=True)
    back_proj = jnp.dot(full_direction, factor_f.T, precision=highest)
    row_squares = lax.psum(jnp.sum(back_proj * back_proj, axis=1), "tp")
    value_step = back_proj / jnp.sqrt(row_squares / WIDTH + 0.01)[:, None]
    new_value = value_weight - 0.05 * value_step
    value_copy = new_value.astype(jnp.bfloat16)
    token_count = glu_output.shape[0]
    reach = kernel.shape[0] - 1
    halo_rows = from_behind(glu_output[token_count - reach :], "fs", 1)
    extended = jnp.concatenate([halo_rows, glu_output], axis=0).astype(jnp.float32)
    cotangent_f = conv_cotangent.astype(jnp.float32)
    pieces = []
    for offset in range(kernel.shape[0]):
        begin = reach - offset
        pieces.append(jnp.sum(extended[begin : begin + token_count] * cotangent_f, axis=0))
    local_grad = jnp.stack(pieces, axis=0)
    kernel_grad = lax.psum(local_grad, "fs")
    new_kernel_first = 0.8 * kernel_first + 0.2 * kernel_grad
    new_kernel_second = 0.9 * kernel_second + 0.1 * kernel_grad * kernel_grad
    new_kernel = kernel - 0.05 * new_kernel_first / jnp.sqrt(new_kernel_second)
    return (
        new_value,
        value_copy,
        value_step,
        new_first,
        new_second,
        new_kernel,
        new_kernel_first,
        new_kernel_second,
    )


def solution(mesh):
    placed = (
        P("fs", "tp"),
        P("fs", None),
        P("fs", "tp"),
        P("fs", "tp"),
        P("tp", None),
        P("fs", "tp"),
        P("fs", "tp"),
        P("fs", "tp"),
        P(None, "tp"),
        P(None, "tp"),
        P(None, "tp"),
    )
    return jax.shard_map(
        body,
        mesh=mesh,
        in_specs=placed,
        out_specs=(
            P("fs", "tp"),
            P("fs", "tp"),
            P("fs", "tp"),
            P("fs", "tp"),
            P("fs", "tp"),
            P(None, "tp"),
            P(None, "tp"),
            P(None, "tp"),
        ),
        check_vma=False,
    )
```

profile of v0, /device:TPU:0, one launch (start us, length us, event | category | flops | bytes accessed | tf_op | source)
XLA Modules:
  0.0 225.3 jit_solution(7543839092658024599)
XLA Ops:
  8.0 0.0 copy-start
  8.0 0.0 reduce-scatter.7.cloned.1.call-start
  8.1 0.9 slice.96
  9.0 4.9 %collective-permute-start = (bf16[30,1024]{1,0:T(8,128)(2,1)S(1)}, bf16[30,1024]{1,0:T(8,128)(2,1)S(1)}, u32[]{:S(2)}, u32[]{:S(2)}) collective-permute-start(bf16[30,1024]{1,0:T(8,128)(2,1)S(1)} %slice.96), channel_id=1, source_target_pairs={{0,2},{2,4},{4,6},{6,8},{8,10},{10,12},{12,14},{14,16},{16,18},{18... | collective-permute-start | bytes 184328 | tf_op jit(solution)/shard_map/ppermute | solution.py:12
  13.9 0.0 copy-done
  13.9 0.0 copy-start.4
  13.9 1.4 convolution_convert_fusion
  15.3 0.7 copy.27
  16.0 0.0 reduce-scatter.7.cloned.1.call-update
  16.1 0.0 copy-start.3
  16.1 0.0 all-reduce.2.cloned.1.call-start
  16.1 0.0 collective-permute-done
  16.1 0.0 copy-done.4
  16.1 0.1 maximum_convert_fusion
  16.2 0.8 copy-done.3
  17.0 1.1 fusion.31
  18.1 0.8 fusion.30
  18.9 0.0 copy-start.1
  18.9 2.7 %stack.127 = f32[31,1024]{1,0:T(8,128)} concatenate(f32[1,1024]{1,0:T(1,128)S(1)} %bitcast.75, f32[1,1024]{1,0:T(1,128)S(1)} %bitcast.46, f32[1,1024]{1,0:T(1,128)S(1)} %bitcast.47, f32[1,1024]{1,0:T(1,128)S(1)} %bitcast.48, f32[1,1024]{1,0:T(1,128)S(1)} %bitcast.49, f32[1,1024]{1,0:T(1,128)S(1)} %bitcast.50, f32[1,1024]{1,0:T(1,128)S(1)} %bitcast.51, f32[1,1024]{1,0:T(1,128)S(1)} %bitcast.52, ...), dimensions={0} | concatenate | bytes 253952 | tf_op jit(solution)/shard_map/stack | solution.py:62
  21.6 0.0 all-reduce.2.cloned.1.call-update
  21.6 0.0 reduce-scatter.5.cloned.1.call-start
  21.7 2.4 %reduce-scatter.7.cloned.1.call-done = bf16[128,128]{1,0:T(8,128)(2,1)} async-done(((bf16[256,128]{1,0:T(8,128)(2,1)}), bf16[128,128]{1,0:T(8,128)(2,1)}) %reduce-scatter.7.cloned.1.call-update) | async-done | bytes 32784
  24.1 0.0 copy-start.8
  24.1 0.9 copy.28
  25.0 0.0 copy-done.1
  25.0 0.0 copy-done.8
  25.0 0.3 fusion.34
  25.3 1.3 fusion
  26.6 0.0 copy-start.9
  26.6 0.0 copy-start.10
  26.6 0.0 copy-start.7
  26.6 0.0 reduce-scatter.5.cloned.1.call-update
  26.6 0.8 copy-done.9
  27.5 0.0 copy-start.5
  27.5 0.0 copy-start.6
  27.5 0.1 copy.24
  27.6 0.0 copy-done.10
  27.6 0.1 copy.23
  27.7 100.1 %all-reduce.2.cloned.1.call-done = f32[31,1024]{1,0:T(8,128)} async-done(((f32[31,1024]{1,0:T(8,128)}), f32[31,1024]{1,0:T(8,128)}) %all-reduce.2.cloned.1.call-update) | async-done | bytes 126992 | tf_op jit(solution)/shard_map/psum | solution.py:63
  127.7 0.0 copy-done.7
  127.7 0.0 copy-done.5
  127.7 0.0 copy-done.6
  127.7 1.7 multiply_subtract_fusion.1
  129.4 78.8 %reduce-scatter.5.cloned.1.call-done = f32[128,128]{0,1:T(8,128)} async-done(((f32[2048,128]{0,1:T(8,128)}), f32[128,128]{0,1:T(8,128)}) %reduce-scatter.5.cloned.1.call-update) | async-done | bytes 65552 | tf_op jit(solution)/shard_map/reduce_scatter | solution.py:43
  208.2 0.9 rsqrt_multiply_fusion
  209.1 1.9 all_gather.3
  211.0 0.0 copy-start.2
  211.0 1.1 multiply_reduce_fusion
  212.1 2.5 %psum.14 = f32[128]{0:T(128)S(1)} all-reduce(f32[128]{0:T(128)S(1)} %get-tuple-element.64), channel_id=1, replica_groups=mesh['fs'=16,'tp'=2] {'tp'}, use_global_device_ids=true, to_apply=%region_3.0 | all-reduce | flops 128 | bytes 1024 | tf_op jit(solution)/shard_map/psum | solution.py:49
  214.5 0.7 copy.25
  215.3 0.7 copy.26
  216.0 0.0 copy-done.2
  216.0 1.8 fusion.37
  (1 shorter events, 0.0 us)
Async XLA Ops:
  8.0 5.9 %copy-start = (bf16[2048,256]{1,0:T(8,128)(2,1)S(1)}, bf16[2048,256]{1,0:T(8,128)(2,1)}, u32[]{:S(2)}) copy-start(bf16[2048,256]{1,0:T(8,128)(2,1)} %param.15) | copy-start | bytes 3145732
  8.0 16.1 %reduce-scatter.7.cloned.1.call-start = ((), (), s32[]{:S(2)}) async-start(), calls=%async_computation.4 | async-start | bytes 98304
  9.0 7.1 %collective-permute-start = (bf16[30,1024]{1,0:T(8,128)(2,1)S(1)}, bf16[30,1024]{1,0:T(8,128)(2,1)S(1)}, u32[]{:S(2)}, u32[]{:S(2)}) collective-permute-start(bf16[30,1024]{1,0:T(8,128)(2,1)S(1)} %slice.96), channel_id=1, source_target_pairs={{0,2},{2,4},{4,6},{6,8},{8,10},{10,12},{12,14},{14,16},{16,18},{18... | collective-permute-start | bytes 184328 | tf_op jit(solution)/shard_map/ppermute | solution.py:12
  13.9 2.2 copy-start.4
  16.1 1.0 copy-start.3
  16.1 111.7 %all-reduce.2.cloned.1.call-start = ((), (), s32[]{:S(2)}) async-start(), calls=%async_computation.3 | async-start | bytes 262144 | tf_op jit(solution)/shard_map/psum | solution.py:63
  18.9 6.1 %copy-start.1 = (bf16[128,2048]{1,0:T(8,128)(2,1)S(1)}, bf16[128,2048]{1,0:T(8,128)(2,1)}, u32[]{:S(2)}) copy-start(bf16[128,2048]{1,0:T(8,128)(2,1)} %param.12) | copy-start | bytes 1572868
  21.6 186.6 %reduce-scatter.5.cloned.1.call-start = ((), (), s32[]{:S(2)}) async-start(), calls=%async_computation.2 | async-start | bytes 1114112 | tf_op jit(solution)/shard_map/reduce_scatter | solution.py:43
  24.1 1.0 copy-start.8
  26.6 0.8 copy-start.9
  26.6 0.9 copy-start.10
  26.6 101.1 %copy-start.7 = (f32[31,1024]{1,0:T(8,128)S(1)}, f32[31,1024]{1,0:T(8,128)}, u32[]{:S(2)}) copy-start(f32[31,1024]{1,0:T(8,128)} %param.21) | copy-start | bytes 380932
  27.5 100.3 %copy-start.5 = (f32[31,1024]{1,0:T(8,128)S(1)}, f32[31,1024]{1,0:T(8,128)}, u32[]{:S(2)}) copy-start(f32[31,1024]{1,0:T(8,128)} %param.19) | copy-start | bytes 380932
  27.5 100.3 %copy-start.6 = (f32[31,1024]{1,0:T(8,128)S(1)}, f32[31,1024]{1,0:T(8,128)}, u32[]{:S(2)}) copy-start(f32[31,1024]{1,0:T(8,128)} %param.20) | copy-start | bytes 380932
  211.0 5.0 %copy-start.2 = (f32[128,2048]{1,0:T(8,128)S(1)}, f32[128,2048]{1,0:T(8,128)}, u32[]{:S(2)}) copy-start(f32[128,2048]{1,0:T(8,128)} %param.16) | copy-start | bytes 3145732
Sparse Core Ops, SparseCore 0:
  16.2 7.8 reduce-scatter.6
Sparse Core Ops, SparseCore 1:
  22.6 105.1 all-reduce.1
  130.4 77.7 reduce-scatter.4
where the time goes:
time: 226 us; the launch traced here: 225 us
  waiting for transfers between devices  181 us (80%)
  between operations  15.6 us (7%)
  local copies, waits for them, and re-layouts  8.54 us (4%)
  other arithmetic  6.33 us (3%)
  starting transfers between devices  5 us (2%)
  blocking collectives  4.37 us (2%)
  matrix products  4.05 us (2%)
    psum x1, waiting for transfers between devices, body(): kernel_grad = lax.psum(local_grad, 'fs')  100 us
    reduce_scatter x1, waiting for transfers between devices, body(): lax.psum_scatter(upper_term + lower_term, 'fs', scatter_dimension=0, tile...  78.8 us
    unnamed x28, local copies, waits for them, and re-layouts  4.95 us
    ppermute x1, starting transfers between devices, from_behind(): return lax.ppermute(x, axis, pairs)  4.87 us
  transfers between devices with their start and end apart: 4, of which 3 were waited for; matrix products, arithmetic and copies ran while one was open for 5% of the time, Pallas kernels for 0%

commit v1 on v0

--- a/solution.py
+++ b/solution.py
@@ -60,7 +60,7 @@
         begin = reach - offset
         pieces.append(jnp.sum(extended[begin : begin + token_count] * cotangent_f, axis=0))
     local_grad = jnp.stack(pieces, axis=0)
-    kernel_grad = lax.psum(local_grad, "fs")
+    kernel_grad = jnp.sum(lax.all_gather(local_grad, "fs"), axis=0)
     new_kernel_first = 0.8 * kernel_first + 0.2 * kernel_grad
     new_kernel_second = 0.9 * kernel_second + 0.1 * kernel_grad * kernel_grad
     new_kernel = kernel - 0.05 * new_kernel_first / jnp.sqrt(new_kernel_second)

time: 226 us -> 174 us (0.77)
  waiting for transfers between devices: 181 us -> 132 us
    psum x1 -> x0, waiting for transfers between devices: 100 us -> none  [body(): kernel_grad = lax.psum(local_grad, 'fs')]
    all_gather x0 -> x1, waiting for transfers between devices: none -> 50.5 us  [body(): kernel_grad = jnp.sum(lax.all_gather(local_grad, 'fs'), axis=0)]
    reduce_scatter x1, waiting for transfers between devices: 78.8 us -> 69.5 us  [body(): lax.psum_scatter(upper_term + lower_term, 'fs', scatter_dimension=0, tile...]
    unnamed x4, waiting for transfers between devices: 2.46 us -> 10.5 us
    unnamed x28 -> x26, local copies, waits for them, and re-layouts: 4.95 us -> 4.44 us
  transfers between devices with their start and end apart: 4 -> 4, of which waited for: 3 -> 4; matrix products, arithmetic and copies ran while one was open for 5% -> 6% of each run, Pallas kernels for 0% -> 0%
where the time goes in v1:
time: 174 us; the launch traced here: 173 us
  waiting for transfers between devices  132 us (76%)
  between operations  13.9 us (8%)
  other arithmetic  7.16 us (4%)
  local copies, waits for them, and re-layouts  7.12 us (4%)
  matrix products  4.77 us (3%)
  blocking collectives  4.35 us (2%)
  starting transfers between devices  3.71 us (2%)
    reduce_scatter x1, waiting for transfers between devices, body(): lax.psum_scatter(upper_term + lower_term, 'fs', scatter_dimension=0, tile...  69.5 us
    all_gather x1, waiting for transfers between devices, body(): kernel_grad = jnp.sum(lax.all_gather(local_grad, 'fs'), axis=0)  50.5 us
    unnamed x4, waiting for transfers between devices  10.5 us
    unnamed x26, local copies, waits for them, and re-layouts  4.44 us
    ppermute x1, starting transfers between devices, from_behind(): return lax.ppermute(x, axis, pairs)  3.58 us
  transfers between devices with their start and end apart: 4, of which 4 were waited for; matrix products, arithmetic and copies ran while one was open for 6% of the time, Pallas kernels for 0%

profile of v1, /device:TPU:0, one launch (start us, length us, event | category | flops | bytes accessed | tf_op | source)
XLA Modules:
  0.0 173.5 jit_solution(16806347754292297058)
XLA Ops:
  7.2 0.0 copy-start
  7.2 0.0 copy-start.1
  7.2 0.0 reduce-scatter.7.cloned.1.call-start
  7.2 1.2 copy-done
  8.4 1.3 convolution_convert_fusion
  9.8 0.7 copy.27
  10.5 0.0 reduce-scatter.7.cloned.1.call-update
  10.5 0.0 reduce-scatter.5.cloned.1.call-start
  10.6 10.5 %reduce-scatter.7.cloned.1.call-done = bf16[128,128]{1,0:T(8,128)(2,1)} async-done(((bf16[256,128]{1,0:T(8,128)(2,1)}), bf16[128,128]{1,0:T(8,128)(2,1)}) %reduce-scatter.7.cloned.1.call-update) | async-done | bytes 32784
  21.1 0.9 copy.28
  21.9 0.0 copy-done.1
  21.9 1.0 fusion.34
  23.0 0.0 copy-start.4
  23.0 0.0 copy-start.3
  23.0 1.3 fusion
  24.3 0.0 reduce-scatter.5.cloned.1.call-update
  24.3 0.0 all-gather.4.cloned.1.call-start
  24.4 0.0 copy-done.4
  24.4 3.6 %collective-permute-start = (bf16[30,1024]{1,0:T(8,128)(2,1)S(1)}, bf16[30,1024]{1,0:T(8,128)(2,1)S(1)}, u32[]{:S(2)}, u32[]{:S(2)}) collective-permute-start(bf16[30,1024]{1,0:T(8,128)(2,1)S(1)} %slice.96), channel_id=1, source_target_pairs={{0,2},{2,4},{4,6},{6,8},{8,10},{10,12},{12,14},{14,16},{16,18},{18... | collective-permute-start | bytes 184328 | tf_op jit(solution)/shard_map/ppermute | solution.py:12
  28.0 1.9 %collective-permute-done = bf16[30,1024]{1,0:T(8,128)(2,1)S(1)} collective-permute-done((bf16[30,1024]{1,0:T(8,128)(2,1)S(1)}, bf16[30,1024]{1,0:T(8,128)(2,1)S(1)}, u32[]{:S(2)}, u32[]{:S(2)}) %collective-permute-start) | collective-permute-done | bytes 61472 | tf_op jit(solution)/shard_map/ppermute | solution.py:12
  29.9 0.1 maximum_convert_fusion
  30.0 0.0 copy-done.3
  30.0 0.8 fusion.30
  30.8 0.0 copy-start.8
  30.8 0.0 copy-start.9
  30.8 1.1 fusion.31
  31.9 0.0 copy-start.2
  31.9 2.7 %stack.127 = f32[31,1024]{1,0:T(8,128)} concatenate(f32[1,1024]{1,0:T(1,128)S(1)} %bitcast.59, f32[1,1024]{1,0:T(1,128)S(1)} %bitcast.61, f32[1,1024]{1,0:T(1,128)S(1)} %bitcast.62, f32[1,1024]{1,0:T(1,128)S(1)} %bitcast.63, f32[1,1024]{1,0:T(1,128)S(1)} %bitcast.64, f32[1,1024]{1,0:T(1,128)S(1)} %bitcast.65, f32[1,1024]{1,0:T(1,128)S(1)} %bitcast.66, f32[1,1024]{1,0:T(1,128)S(1)} %bitcast.67, ...), dimensions={0} | concatenate | bytes 253952 | tf_op jit(solution)/shard_map/stack | solution.py:62
  34.6 0.0 all-gather.4.cloned.1.call-update
  34.6 0.0 copy-done.8
  34.6 0.1 copy.23
  34.7 0.0 copy-done.9
  34.7 0.1 copy.24
  34.8 69.5 %reduce-scatter.5.cloned.1.call-done = f32[128,128]{0,1:T(8,128)} async-done(((f32[2048,128]{0,1:T(8,128)}), f32[128,128]{0,1:T(8,128)}) %reduce-scatter.5.cloned.1.call-update) | async-done | bytes 65552 | tf_op jit(solution)/shard_map/reduce_scatter | solution.py:43
  104.3 0.9 rsqrt_multiply_fusion
  105.2 0.7 copy.26
  105.9 0.7 copy.25
  106.7 1.9 %all_gather.9 = f32[128,256]{0,1:T(8,128)S(1)} all-gather(f32[128,128]{0,1:T(8,128)S(1)} %get-tuple-element.61), channel_id=1, replica_groups=mesh['fs'=16,'tp'=2] {'tp'}, dimensions={1}, use_global_device_ids=true | all-gather | bytes 196608 | tf_op jit(solution)/shard_map/all_gather | solution.py:47
  108.6 1.1 multiply_reduce_fusion
  109.6 2.5 %psum.7 = f32[128]{0:T(128)S(1)} all-reduce(f32[128]{0:T(128)S(1)} %get-tuple-element.64), channel_id=1, replica_groups=mesh['fs'=16,'tp'=2] {'tp'}, use_global_device_ids=true, to_apply=%region_3.0 | all-reduce | flops 128 | bytes 1024 | tf_op jit(solution)/shard_map/psum | solution.py:49
  112.1 0.0 copy-done.2
  112.1 1.8 %fusion.37 = (bf16[128,2048]{1,0:T(8,128)(2,1)}, f32[128,2048]{1,0:T(8,128)}, f32[128,2048]{1,0:T(8,128)}) fusion(f32[128,2048]{1,0:T(8,128)S(1)} %copy-done.2, f32[128,2048]{1,0:T(8,128)S(1)} %get-tuple-element.65, f32[128]{0:T(128)S(1)} %add_sqrt_fusion), kind=kLoop, calls=%fused_computation.81 | loop fusion | flops 1048576 | bytes 4719104 | tf_op jit(solution)/shard_map/convert_element_type | solution.py:52
  114.0 0.0 copy-start.5
  114.0 0.0 copy-start.6
  114.0 0.0 copy-start.7
  114.0 50.5 %all-gather.4.cloned.1.call-done = f32[16,31,1024]{2,1,0:T(8,128)} async-done(((f32[1,31,1024]{2,1,0:T(8,128)}), f32[16,31,1024]{2,1,0:T(8,128)}) %all-gather.4.cloned.1.call-update) | async-done | bytes 2031632 | tf_op jit(solution)/shard_map/all_gather | solution.py:63
  164.4 1.7 reduce_sum.329
  166.2 0.0 copy-done.5
  166.2 0.0 copy-done.6
  166.2 0.0 copy-done.7
  166.2 0.8 multiply_subtract_fusion.1
  (2 shorter events, 0.0 us)
Async XLA Ops:
  7.2 1.2 copy-start
  7.2 14.7 %copy-start.1 = (bf16[128,2048]{1,0:T(8,128)(2,1)S(1)}, bf16[128,2048]{1,0:T(8,128)(2,1)}, u32[]{:S(2)}) copy-start(bf16[128,2048]{1,0:T(8,128)(2,1)} %param.12) | copy-start | bytes 1572868
  7.2 13.9 %reduce-scatter.7.cloned.1.call-start = ((), (), s32[]{:S(2)}) async-start(), calls=%async_computation.4 | async-start | bytes 98304
  10.5 93.8 %reduce-scatter.5.cloned.1.call-start = ((), (), s32[]{:S(2)}) async-start(), calls=%async_computation.2 | async-start | bytes 1114112 | tf_op jit(solution)/shard_map/reduce_scatter | solution.py:43
  23.0 1.4 copy-start.4
  23.0 7.0 %copy-start.3 = (bf16[128,1024]{1,0:T(8,128)(2,1)S(1)}, bf16[128,1024]{1,0:T(8,128)(2,1)}, u32[]{:S(2)}) copy-start(bf16[128,1024]{1,0:T(8,128)(2,1)} %param.14) | copy-start | bytes 786436
  24.3 140.1 %all-gather.4.cloned.1.call-start = ((), (), s32[]{:S(2)}) async-start(), calls=%async_computation.3 | async-start | bytes 2228224 | tf_op jit(solution)/shard_map/all_gather | solution.py:63
  24.4 5.5 %collective-permute-start = (bf16[30,1024]{1,0:T(8,128)(2,1)S(1)}, bf16[30,1024]{1,0:T(8,128)(2,1)S(1)}, u32[]{:S(2)}, u32[]{:S(2)}) collective-permute-start(bf16[30,1024]{1,0:T(8,128)(2,1)S(1)} %slice.96), channel_id=1, source_target_pairs={{0,2},{2,4},{4,6},{6,8},{8,10},{10,12},{12,14},{14,16},{16,18},{18... | collective-permute-start | bytes 184328 | tf_op jit(solution)/shard_map/ppermute | solution.py:12
  30.8 3.8 %copy-start.8 = (f32[128,128]{1,0:T(8,128)S(1)}, f32[128,128]{1,0:T(8,128)}, u32[]{:S(2)}) copy-start(f32[128,128]{1,0:T(8,128)} %param.17) | copy-start | bytes 196612
  30.8 3.9 %copy-start.9 = (f32[128,128]{1,0:T(8,128)S(1)}, f32[128,128]{1,0:T(8,128)}, u32[]{:S(2)}) copy-start(f32[128,128]{1,0:T(8,128)} %param.18) | copy-start | bytes 196612
  31.9 80.2 %copy-start.2 = (f32[128,2048]{1,0:T(8,128)S(1)}, f32[128,2048]{1,0:T(8,128)}, u32[]{:S(2)}) copy-start(f32[128,2048]{1,0:T(8,128)} %param.16) | copy-start | bytes 3145732
  114.0 52.2 %copy-start.5 = (f32[31,1024]{1,0:T(8,128)S(1)}, f32[31,1024]{1,0:T(8,128)}, u32[]{:S(2)}) copy-start(f32[31,1024]{1,0:T(8,128)} %param.19) | copy-start | bytes 380932
  114.0 52.2 %copy-start.6 = (f32[31,1024]{1,0:T(8,128)S(1)}, f32[31,1024]{1,0:T(8,128)}, u32[]{:S(2)}) copy-start(f32[31,1024]{1,0:T(8,128)} %param.20) | copy-start | bytes 380932
  114.0 52.2 %copy-start.7 = (f32[31,1024]{1,0:T(8,128)S(1)}, f32[31,1024]{1,0:T(8,128)}, u32[]{:S(2)}) copy-start(f32[31,1024]{1,0:T(8,128)} %param.21) | copy-start | bytes 380932
Sparse Core Ops, SparseCore 0:
  10.8 10.2 reduce-scatter.6
  24.4 79.8 reduce-scatter.4
  107.7 56.6 all-gather.3
